TPU v7x, 32 devices: a whole 2x2x4 slice. The times are simulated.
32 devices in a mesh: fs: 8 (over z, y), tp: 4 (over x, core).
Axes of the slice: x: 2, y: 2, z: 4, core: 2. Of those that a mesh axis runs over, the one named last changes fastest.
Arguments:
- tokens: bfloat16 [6144, 2048], P('fs'), may hold values from -6 to 6
- norm_gain: float32 [2048], P('fs'), may hold values from 0.1 to 1.9
- gate_weight: float32 [2048, 5632], P('fs', 'tp'), may hold values from -0.125 to 0.125
- up_weight: float32 [2048, 5632], P('fs', 'tp'), may hold values from -0.125 to 0.125
- down_weight: float32 [5632, 2048], P('fs', 'tp'), may hold values from -0.078125 to 0.078125
Outputs:
- gate_out: bfloat16 [2048, 5632], P(None, 'tp')
- up_out: bfloat16 [2048, 5632], P(None, 'tp')
- down_out: bfloat16 [5632, 2048], P('tp')
- mixed: bfloat16 [6144, 2048], P('fs', 'tp')
All inputs are finite; a program needn't handle non-finite values.
Results may differ from a plain program's by a relative error of at most 0.0095.
Values may be sent and summed in bfloat16 or wider, within the bound.
A program may use at most 128 MiB of HBM per device.

v0:
```python
import jax
import jax.numpy as jnp
from jax import lax
from jax.sharding import PartitionSpec as P

eps_norm = 1e-06


def on_device(tokens, norm_gain, gate_weight, up_weight, down_weight):
    gain_column = norm_gain[:, None]
    gate_cast = (gate_weight * gain_column).astype(jnp.bfloat16)
    up_cast = (up_weight * gain_column).astype(jnp.bfloat16)
    down_cast = down_weight.astype(jnp.bfloat16)
    gate_out, up_out = (
        lax.all_gather(gate_cast, "fs", axis=0, tiled=True),
        lax.all_gather(up_cast, "fs", axis=0, tiled=True),
    )
    column_block = lax.all_gather(down_cast, "fs", axis=0, tiled=True)
    down_out = lax.all_to_all(column_block, "tp", split_axis=0, concat_axis=1, tiled=True)
    rows_float = tokens.astype(jnp.float32)
    normed = (
        rows_float * lax.rsqrt(jnp.mean(rows_float * rows_float, axis=-1, keepdims=True) + eps_norm)
    ).astype(jnp.bfloat16)
    gate_act = jnp.dot(normed, gate_out, preferred_element_type=jnp.float32)
    up_act = jnp.dot(normed, up_out, preferred_element_type=jnp.float32)
    hidden = (jax.nn.silu(gate_act) * up_act).astype(jnp.bfloat16)
    share = jnp.dot(hidden, down_out, preferred_element_type=jnp.float32).astype(jnp.bfloat16)
    share = lax.optimization_barrier(share).astype(jnp.float32)
    summed = lax.psum_scatter(share.astype(jnp.bfloat16), "tp", scatter_dimension=1, tiled=True)
    return (gate_out, up_out, down_out, summed)


def solution(mesh):
    in_specs = (P("fs", None), P("fs"), P("fs", "tp"), P("fs", "tp"), P("fs", "tp"))
    out_specs = (P(None, "tp"), P(None, "tp"), P("tp", None), P("fs", "tp"))
    return jax.shard_map(
        on_device, mesh=mesh, in_specs=in_specs, out_specs=out_specs, check_vma=False
    )
```

profile of v0, /device:TPU:0, one launch (start us, length us, event | category | flops | bytes accessed | tf_op | source)
XLA Modules:
  0.0 363.5 jit_solution(17786018293957945412)
XLA Ops:
  7.2 0.0 all-gather.8.cloned.1.call-start
  7.2 2.3 convert_element_type.25
  9.5 0.0 all-gather.8.cloned.1.call-update
  9.5 0.0 all-gather.4.cloned.1.call-start
  9.6 3.2 multiply_convert_fusion.1
  12.8 0.0 all-gather.4.cloned.1.call-update
  12.8 0.0 all-gather.6.cloned.1.call-start
  12.8 0.7 all-gather.6.cloned.1.call-update
  13.5 92.3 %all-gather.8.cloned.1.call-done = bf16[5632,512]{1,0:T(8,128)(2,1)} async-done(((bf16[704,512]{1,0:T(8,128)(2,1)}), bf16[5632,512]{1,0:T(8,128)(2,1)}) %all-gather.8.cloned.1.call-update) | async-done | bytes 5767184 | tf_op jit(solution)/shard_map/all_gather | solution.py:18
  105.8 5.4 %all-to-all-start = ((bf16[4,1408,512]{2,1,0:T(8,128)(2,1)}), bf16[4,1408,512]{2,1,0:T(8,128)(2,1)}, u32[]{:S(2)}, u32[]{:S(2)}) async-start(bf16[4,1408,512]{2,1,0:T(8,128)(2,1)} %bitcast.9), calls=%async_computation | async-start | bytes 11534336 | tf_op jit(solution)/shard_map/all_to_all | solution.py:19
  111.2 0.0 reduce-scatter.2.cloned.1.call-start
  111.3 0.0 copy-done
  111.3 0.7 fusion
  112.0 87.1 %all-gather.4.cloned.1.call-done = bf16[2048,1408]{1,0:T(8,128)(2,1)} async-done(((bf16[256,1408]{1,0:T(8,128)(2,1)}), bf16[2048,1408]{1,0:T(8,128)(2,1)}) %all-gather.4.cloned.1.call-update) | async-done | bytes 5767184 | tf_op jit(solution)/shard_map/all_gather | solution.py:15
  199.1 9.4 %fusion.3 = f32[768,1408]{1,0:T(8,128)} fusion(bf16[2048,1408]{1,0:T(8,128)(2,1)} %all-gather.4.cloned.1.call-done, bf16[768,2048]{1,0:T(8,128)(2,1)S(1)} %copy-done, f32[768]{0:T(1024)S(1)} %add_rsqrt_fusion), kind=kOutput, calls=%fused_computation.8 | convolution fusion | flops 4433903616 | bytes 13241344 | tf_op jit(solution)/shard_map/dot_general | solution.py:24
  208.4 0.0 all-to-all-done
  208.4 8.4 %copy.10 = bf16[4,1408,512]{1,2,0:T(8,128)(2,1)} copy(bf16[4,1408,512]{2,1,0:T(8,128)(2,1)} %all-to-all-done) | data formatting | bytes 11534336 | tf_op jit(solution)/shard_map/all_to_all | solution.py:19
  216.8 75.6 %all-gather.6.cloned.1.call-done = bf16[2048,1408]{1,0:T(8,128)(2,1)} async-done(((bf16[256,1408]{1,0:T(8,128)(2,1)}), bf16[2048,1408]{1,0:T(8,128)(2,1)}) %all-gather.6.cloned.1.call-update) | async-done | bytes 5767184 | tf_op jit(solution)/shard_map/all_gather | solution.py:16
  292.4 17.3 %convolution_convert_fusion = bf16[768,2048]{1,0:T(8,128)(2,1)} fusion(bf16[1408,2048]{0,1:T(8,128)(2,1)} %bitcast.7, f32[768,1408]{1,0:T(8,128)} %fusion.3, bf16[2048,1408]{1,0:T(8,128)(2,1)} %all-gather.6.cloned.1.call-done, bf16[768,2048]{1,0:T(8,128)(2,1)S(1)} %copy-done, f32[768]{0:T(1024)S(1)} %add_rsqrt_fusion), kind=kOutput, calls=%fused_computation.5 | convolution fusion | flops 8871149568 | bytes 22154240 | tf_op jit(solution)/shard_map/dot_general | solution.py:27
  309.7 0.0 reduce-scatter.2.cloned.1.call-update
  309.7 8.4 %copy.11 = bf16[1408,2048]{1,0:T(8,128)(2,1)} copy(bf16[1408,2048]{0,1:T(8,128)(2,1)} %bitcast.8) | data formatting | bytes 11534336
  318.2 27.6 %reduce-scatter.2.cloned.1.call-done = bf16[768,512]{1,0:T(8,128)(2,1)} async-done(((bf16[768,2048]{1,0:T(8,128)(2,1)}), bf16[768,512]{1,0:T(8,128)(2,1)}) %reduce-scatter.2.cloned.1.call-update) | async-done | bytes 786448 | tf_op jit(solution)/shard_map/reduce_scatter | solution.py:29
  345.7 5.6 %copy.14 = bf16[2048,1408]{1,0:T(8,128)(2,1)} copy(bf16[2048,1408]{1,0:T(8,128)(2,1)} %all-gather.4.cloned.1.call-done) | data formatting | bytes 11534336
  351.3 5.6 %copy.15 = bf16[2048,1408]{1,0:T(8,128)(2,1)} copy(bf16[2048,1408]{1,0:T(8,128)(2,1)} %all-gather.6.cloned.1.call-done) | data formatting | bytes 11534336
  (2 shorter events, 0.0 us)
Async XLA Ops:
  7.2 98.6 %all-gather.8.cloned.1.call-start = ((), (), s32[]{:S(2)}) async-start(), calls=%async_computation.4 | async-start | bytes 6488064 | tf_op jit(solution)/shard_map/all_gather | solution.py:18
  9.5 189.5 %all-gather.4.cloned.1.call-start = ((), (), s32[]{:S(2)}) async-start(), calls=%async_computation.2 | async-start | bytes 6488064 | tf_op jit(solution)/shard_map/all_gather | solution.py:15
  12.8 279.6 %all-gather.6.cloned.1.call-start = ((), (), s32[]{:S(2)}) async-start(), calls=%async_computation.3 | async-start | bytes 6488064 | tf_op jit(solution)/shard_map/all_gather | solution.py:16
  105.8 5.5 %copy-start = (bf16[768,2048]{1,0:T(8,128)(2,1)S(1)}, bf16[768,2048]{1,0:T(8,128)(2,1)}, u32[]{:S(2)}) copy-start(bf16[768,2048]{1,0:T(8,128)(2,1)} %param.5) | copy-start | bytes 9437188
  105.8 102.6 %all-to-all-start = ((bf16[4,1408,512]{2,1,0:T(8,128)(2,1)}), bf16[4,1408,512]{2,1,0:T(8,128)(2,1)}, u32[]{:S(2)}, u32[]{:S(2)}) async-start(bf16[4,1408,512]{2,1,0:T(8,128)(2,1)} %bitcast.9), calls=%async_computation | async-start | bytes 11534336 | tf_op jit(solution)/shard_map/all_to_all | solution.py:19
  111.2 234.5 %reduce-scatter.2.cloned.1.call-start = ((), (), s32[]{:S(2)}) async-start(), calls=%async_computation.5 | async-start | bytes 3932160 | tf_op jit(solution)/shard_map/reduce_scatter | solution.py:29
Sparse Core Ops, SparseCore 0:
  10.7 95.0 all-gather.7
  108.5 90.4 all-gather.3
  201.8 90.4 all-gather.5
  309.8 35.8 reduce-scatter.1
where the time goes:
time: 364 us; the launch traced here: 363 us
  waiting for transfers between devices  283 us (78%)
  local copies, waits for them, and re-layouts  28 us (8%)
  matrix products  26.7 us (7%)
  between operations  13.8 us (4%)
  other arithmetic  6.17 us (2%)
  starting transfers between devices  5.6 us (2%)
    all_gather x1, waiting for transfers between devices, on_device(): column_block = lax.all_gather(down_cast, 'fs', axis=0, tiled=True)  92.3 us
    all_gather x1, waiting for transfers between devices, on_device(): lax.all_gather(gate_cast, 'fs', axis=0, tiled=True)  87.1 us
    all_gather x1, waiting for transfers between devices, on_device(): lax.all_gather(up_cast, 'fs', axis=0, tiled=True)  75.6 us
    reduce_scatter x1, waiting for transfers between devices, on_device(): lax.psum_scatter(share.astype(jnp.bfloat16), 'tp', scatter_dimension=1, t...  27.6 us
    unnamed x5, local copies, waits for them, and re-layouts  19.6 us
    dot_general x1, matrix products, on_device(): jnp.dot(hidden, down_out, preferred_element_type=jnp.float32)  17.3 us
    dot_general x1, matrix products, on_device(): gate_act = jnp.dot(normed, gate_out, preferred_element_type=jnp.float32)  9.36 us
    all_to_all x1, local copies, waits for them, and re-layouts, on_device(): lax.all_to_all(column_block, 'tp', split_axis=0, concat_axis=1, tiled=True)  8.35 us
  transfers between devices with their start and end apart: 5, of which 4 were waited for; matrix products, arithmetic and copies ran while one was open for 8% of the time, Pallas kernels for 0%

commit v1 on v0

v1 whole, which is shorter than its diff:
```python
import functools

import jax
import jax.numpy as jnp
from jax import lax
from jax.experimental import pallas as pl
from jax.experimental.pallas import tpu as pltpu
from jax.sharding import PartitionSpec as P

eps_norm = 1e-06
MESH = pl.DeviceIdType.MESH

PIECES = (
    ("gate", 0, "a"),
    ("gate", 1, "a"),
    ("down", 1, "b"),
    ("up", 0, "a"),
    ("up", 1, "a"),
    ("down", 0, "a"),
)
PHASES = ((0, 1), (2,), (3, 4), (5,))


def plan(n_z):
    events = []
    seq = [(d, p) for phase in PHASES for d in range(1, n_z) for p in phase]
    own = {p: i + 1.0 for i, p in enumerate(range(len(PIECES)))}
    z_time, now = {}, 0.0
    for phase in PHASES:
        for d in range(1, n_z):
            for p in phase:
                if PIECES[p][2] == "a":
                    now += 1.0
                    z_time[d, p] = now
                    events.append((now, 0, "line", d, p))
                else:
                    now += 2.0
                    z_time[d, p] = now
                    events.append((now - 1.0, 0, "line", d, p))
                    events.append((now, 0, "line_other", d, p))
    y_time = {}
    for z in range(n_z):
        at = float(len(PIECES))
        for d, p in seq:
            if PIECES[p][2] == "a":
                for zz in (z - d, z + d):
                    if 0 <= zz < n_z:
                        at = max(at + 1.0, z_time[d, p] + 1.0)
                        y_time[d, p] = max(y_time.get((d, p), 0.0), at)
    for p, at in own.items():
        events.append((at, 1, "pair", 0, p))
    for (d, p), at in y_time.items():
        events.append((at, 1, "pair", d, p))
    here = dict(y_time)
    here.update({(0, p): at for p, at in own.items()})
    last = 0.0
    for name in ("gate", "up"):
        mine = [p for p in range(len(PIECES)) if PIECES[p][0] == name]
        for d in range(n_z):
            at = max(here[d, p] for p in mine) + 0.01
            events.append((at, 2, "mul_" + name, d, 0))
            last = max(last, at)
    events.append((last + 0.01, 3, "act", 0, 0))
    return sorted(events)


def kernel(
    n_fs, n_tp, tok, gain, gw, uw, dw, gate_o, up_o, down_o, mix_o,
    dcol, normed, acc_g, acc_u, hidden, share, half_in, out_send, out_in,
    ag_send, ag_recv, aa_send, aa_recv, rs_send, rs_recv,
):
    f, t = lax.axis_index("fs"), lax.axis_index("tp")
    n_z = n_fs // 2
    z, y = f // 2, f % 2
    per = n_fs // n_tp
    rows = gw.shape[0]
    d_rows, d_cols = dw.shape
    half = d_cols // 2
    n_tok = tok.shape[0]
    k_z = normed.shape[2]
    m_tile = min(256, n_tok)
    width = gw.shape[1]
    col_tiles = [(c, min(512, width - c)) for c in range(0, width, 512)]

    def flip(bit):
        return t + bit - 2 * bit * ((t // bit) % 2)

    near, far = flip(1), flip(2)
    far_near = far + 1 - 2 * (far % 2)

    def view(o, p):
        name, h, _ = PIECES[p]
        if name == "down":
            return dcol.at[o, :, pl.ds(h * half, half)]
        ref = gate_o if name == "gate" else up_o
        return ref.at[pl.ds(pl.multiple_of(o * rows + h * (rows // 2), rows // 2), rows // 2), :]

    def ag(o, p, way, dest):
        v = view(o, p)
        return pltpu.make_async_remote_copy(
            v, v, ag_send.at[o, p, way], ag_recv.at[o, p],
            device_id=(dest, t), device_id_type=MESH,
        )

    started = []

    def start(cond, make):
        if cond is None:
            make().start()
        else:
            pl.when(cond)(lambda: make().start())
        started.append((cond, make))

    def land(o, p):
        ag(o, p, 0, f).wait_recv()

    def exchange(cond, o, p):
        name, h, _ = PIECES[p]
        if name != "down":
            return
        owner = o // per
        k = o % per
        row = pl.multiple_of(k * d_rows, d_rows)
        col = pl.multiple_of(t * d_cols + h * half, half)

        def make():
            return pltpu.make_async_remote_copy(
                view(o, p), down_o.at[pl.ds(row, d_rows), pl.ds(col, half)],
                aa_send.at[o, h], aa_recv.at[t, k, h],
                device_id=(f, owner), device_id_type=MESH,
            )

        away = owner != t
        start(away if cond is None else jnp.logical_and(cond, away), make)
        mine = owner == t

        @pl.when(mine if cond is None else jnp.logical_and(cond, mine))
        def _():
            down_o[pl.ds(row, d_rows), pl.ds(col, half)] = dcol[o, :, h * half : (h + 1) * half]

    barrier = pltpu.get_barrier_semaphore()
    other_y = f + 1 - 2 * y
    peers = [
        (z > 0, (f - 2, t)), (z < n_z - 1, (f + 2, t)), (None, (other_y, t)),
        (None, (f, near)), (None, (f, far)), (None, (f, far_near)),
    ]
    for cond, dev in peers:
        def hello(dev=dev):
            pl.semaphore_signal(barrier, inc=1, device_id=dev, device_id_type=MESH)
        hello() if cond is None else pl.when(cond)(hello)

    g = gain[...]
    base = pl.multiple_of(f * rows, rows)
    gate_o[pl.ds(base, rows), :] = (gw[...] * g).astype(jnp.bfloat16)
    dcol[f] = dw[...].astype(jnp.bfloat16)
    up_o[pl.ds(base, rows), :] = (uw[...] * g).astype(jnp.bfloat16)
    inner = jnp.logical_and(z > 0, z < n_z - 1)
    pl.when(inner)(lambda: pl.semaphore_wait(barrier, len(peers)))
    pl.when(jnp.logical_not(inner))(lambda: pl.semaphore_wait(barrier, len(peers) - 1))

    for p in range(len(PIECES)):
        start(z > 0, functools.partial(ag, f, p, 0, f - 2))
        start(z < n_z - 1, functools.partial(ag, f, p, 1, f + 2))
        start(None, functools.partial(ag, f, p, 2, other_y))
    for p in range(len(PIECES)):
        exchange(None, f, p)

    n_norm = n_tok // 64

    @pl.loop(0, n_norm)
    def _(i):
        r = pl.multiple_of(i * 64, 64)
        x = tok[pl.ds(r, 64), :].astype(jnp.float32)
        x = x * lax.rsqrt(jnp.mean(x * x, axis=-1, keepdims=True) + eps_norm)
        x = x.astype(jnp.bfloat16)
        for j in range(n_z):
            normed[j, pl.ds(r, 64), :] = x[:, j * k_z : (j + 1) * k_z]

    def multiply(w, acc, zz, first):
        k0 = pl.multiple_of(zz * k_z, k_z)

        @pl.loop(0, n_tok // m_tile)
        def _(i):
            r = pl.multiple_of(i * m_tile, m_tile)
            a = normed[zz, pl.ds(r, m_tile), :]
            for c, n in col_tiles:
                v = jnp.dot(a, w[pl.ds(k0, k_z), c : c + n], preferred_element_type=jnp.float32)
                if first:
                    acc[pl.ds(r, m_tile), c : c + n] = v
                else:
                    acc[pl.ds(r, m_tile), c : c + n] += v

    def sides(d):
        return [(z >= d, z - d, -1), (z + d < n_z, z + d, 1)]

    def forward(cond, zz, sign, o, p):
        if sign < 0:
            start(jnp.logical_and(cond, z < n_z - 1), functools.partial(ag, o, p, 1, f + 2))
        else:
            start(jnp.logical_and(cond, z > 0), functools.partial(ag, o, p, 0, f - 2))

    def halves(h):
        k_tile = 256

        def aa_wait(c):
            for k in range(per):
                pltpu.make_async_remote_copy(
                    down_o.at[pl.ds(k * d_rows, d_rows), pl.ds(0, half)],
                    down_o.at[pl.ds(k * d_rows, d_rows), pl.ds(pl.multiple_of(c * d_cols + h * half, half), half)],
                    aa_send.at[0, h], aa_recv.at[c, k, h], device_id=(f, near), device_id_type=MESH,
                ).wait_recv()

        def product(c, slot):
            @pl.loop(0, n_tok // m_tile)
            def _(i):
                r = pl.multiple_of(i * m_tile, m_tile)
                col = pl.multiple_of(c * d_cols + h * half, half)
                v = jnp.dot(hidden[pl.ds(r, m_tile), :], down_o[:, pl.ds(col, half)], preferred_element_type=jnp.float32)
                share[h, slot, pl.ds(r, m_tile), :] = v.astype(jnp.bfloat16)

        def pair(slot):
            return pltpu.make_async_remote_copy(
                share.at[h, slot], half_in.at[h, slot], rs_send.at[h, slot], rs_recv.at[h, slot],
                device_id=(f, near), device_id_type=MESH,
            )

        def across():
            return pltpu.make_async_remote_copy(
                out_send.at[h], out_in.at[h], rs_send.at[h, 2], rs_recv.at[h, 2],
                device_id=(f, far), device_id_type=MESH,
            )

        aa_wait(far_near)
        product(far_near, 0)
        start(None, functools.partial(pair, 0))
        aa_wait(far)
        product(far, 2)
        pair(0).wait_recv()
        out_send[h] = (share[h, 2].astype(jnp.float32) + half_in[h, 0].astype(jnp.float32)).astype(jnp.bfloat16)
        start(None, across)
        aa_wait(near)
        product(near, 1)
        start(None, functools.partial(pair, 1))
        product(t, 3)

        def finish():
            pair(1).wait_recv()
            across().wait_recv()
            mix_o[:, h * half : (h + 1) * half] = (
                share[h, 3].astype(jnp.float32) + half_in[h, 1].astype(jnp.float32) + out_in[h].astype(jnp.float32)
            ).astype(jnp.bfloat16)

        return finish

    for _, _, what, d, p in plan(n_z):
        if what == "line":
            for cond, zz, sign in sides(d):
                o = zz * 2 + y
                pl.when(cond)(functools.partial(land, o, p))
                forward(cond, zz, sign, o, p)
                if PIECES[p][2] == "a":
                    start(cond, functools.partial(ag, o, p, 2, other_y))
                exchange(cond, o, p)
        elif what == "line_other":
            for cond, zz, sign in sides(d):
                o = zz * 2 + 1 - y
                pl.when(cond)(functools.partial(land, o, p))
                forward(cond, zz, sign, o, p)
                exchange(cond, o, p)
        elif what == "pair":
            if d == 0:
                land(other_y, p)
                if PIECES[p][2] == "b":
                    start(z > 0, functools.partial(ag, other_y, p, 0, f - 2))
                    start(z < n_z - 1, functools.partial(ag, other_y, p, 1, f + 2))
                exchange(None, other_y, p)
            else:
                for cond, zz, sign in sides(d):
                    o = zz * 2 + 1 - y
                    pl.when(cond)(functools.partial(land, o, p))
                    exchange(cond, o, p)
        elif what == "mul_gate" or what == "mul_up":
            w, acc = (gate_o, acc_g) if what == "mul_gate" else (up_o, acc_u)
            if d == 0:
                multiply(w, acc, z, True)
            else:
                for cond, zz, sign in sides(d):
                    pl.when(cond)(functools.partial(multiply, w, acc, zz, False))
        elif what == "act":
            @pl.loop(0, n_tok // 32)
            def _(i):
                r = pl.multiple_of(i * 32, 32)
                v = acc_g[pl.ds(r, 32), :]
                hidden[pl.ds(r, 32), :] = (v / (1.0 + jnp.exp(-v)) * acc_u[pl.ds(r, 32), :]).astype(jnp.bfloat16)

    first = halves(1)
    second = halves(0)
    first()
    second()
    for cond, make in started:
        if cond is None:
            make().wait_send()
        else:
            pl.when(cond)(lambda make=make: make().wait_send())


def on_device(n_fs, n_tp, tokens, norm_gain, gate_weight, up_weight, down_weight):
    n_tok, d_model = tokens.shape
    rows, width = gate_weight.shape
    d_rows, d_cols = down_weight.shape
    half = d_cols // 2
    n_z = n_fs // 2
    n_p = len(PIECES)
    bf = jnp.bfloat16
    vmem = pl.BlockSpec(memory_space=pltpu.VMEM)
    dma = pltpu.SemaphoreType.DMA
    return pl.pallas_call(
        functools.partial(kernel, n_fs, n_tp),
        out_shape=(
            jax.ShapeDtypeStruct((d_model, width), bf),
            jax.ShapeDtypeStruct((d_model, width), bf),
            jax.ShapeDtypeStruct((d_rows * n_fs // n_tp, d_model), bf),
            jax.ShapeDtypeStruct((n_tok, d_cols), bf),
        ),
        in_specs=[vmem] * 5,
        out_specs=(vmem,) * 4,
        scratch_shapes=[
            pltpu.VMEM((n_fs, d_rows, d_cols), bf),
            pltpu.VMEM((n_z, n_tok, d_model // n_z), bf),
            pltpu.VMEM((n_tok, width), jnp.float32),
            pltpu.VMEM((n_tok, width), jnp.float32),
            pltpu.VMEM((n_tok, width), bf),
            pltpu.VMEM((2, 4, n_tok, half), bf),
            pltpu.VMEM((2, 2, n_tok, half), bf),
            pltpu.VMEM((2, n_tok, half), bf),
            pltpu.VMEM((2, n_tok, half), bf),
            dma((n_fs, n_p, 3)),
            dma((n_fs, n_p)),
            dma((n_fs, 2)),
            dma((n_tp, n_fs // n_tp, 2)),
            dma((2, 3)),
            dma((2, 3)),
        ],
        compiler_params=pltpu.CompilerParams(
            collective_id=0, has_side_effects=True, vmem_limit_bytes=67043328
        ),
    )(tokens, norm_gain[:, None], gate_weight, up_weight, down_weight)


def solution(mesh):
    n_fs, n_tp = mesh.shape["fs"], mesh.shape["tp"]
    in_specs = (P("fs", None), P("fs"), P("fs", "tp"), P("fs", "tp"), P("fs", "tp"))
    out_specs = (P(None, "tp"), P(None, "tp"), P("tp", None), P("fs", "tp"))
    return jax.shard_map(
        functools.partial(on_device, n_fs, n_tp), mesh=mesh, in_specs=in_specs, out_specs=out_specs, check_vma=False
    )
```

time: 364 us -> 254 us (0.70)
  waiting for transfers between devices: 283 us -> 0 us
  Pallas kernels: 0 us -> 238 us
  matrix products: 26.7 us -> 0 us
  between operations: 13.8 us -> 0.65 us
  local copies, waits for them, and re-layouts: 28 us -> 15.4 us
  other arithmetic: 6.17 us -> 0 us
  starting transfers between devices: 5.6 us -> 0 us
    all_gather x3 -> x0, waiting for transfers between devices: 255 us -> none  [the longest x1 92.3 us: on_device(): column_block = lax.all_gather(down_cast, 'fs', axis=0, tiled=True)]
    pallas_call x0 -> x1, Pallas kernels: none -> 238 us  [on_device(): pl.pallas_call(functools.partial(kernel, n_fs, n_tp), out_shape=(jax.Shap...]
    reduce_scatter x1 -> x0, waiting for transfers between devices: 27.6 us -> none  [on_device(): lax.psum_scatter(share.astype(jnp.bfloat16), 'tp', scatter_dimension=1, t...]
    dot_general x2 -> x0, matrix products: 26.7 us -> none  [the longest x1 17.3 us: on_device(): jnp.dot(hidden, down_out, preferred_element_type=jnp.float32)]
    all_to_all x1 -> x0, local copies, waits for them, and re-layouts: 8.35 us -> none  [on_device(): lax.all_to_all(column_block, 'tp', split_axis=0, concat_axis=1, tiled=True)]
    unnamed x5 -> x10, local copies, waits for them, and re-layouts: 19.6 us -> 13.9 us
    convert_element_type x2 -> x0, other arithmetic: 5.48 us -> none  [the longest x1 3.17 us: on_device(): up_cast = (up_weight * gain_column).astype(jnp.bfloat16)]
    all_to_all x1 -> x0, starting transfers between devices: 5.43 us -> none  [on_device(): lax.all_to_all(column_block, 'tp', split_axis=0, concat_axis=1, tiled=True)]
  transfers between devices with their start and end apart: 5 -> 0, of which waited for: 4 -> 0; matrix products, arithmetic and copies ran while one was open for 8% -> 0% of each run, Pallas kernels for 0% -> 0%
where the time goes in v1:
time: 254 us
  Pallas kernels  238 us (94%)
  local copies, waits for them, and re-layouts  15.4 us (6%)
    pallas_call x1, Pallas kernels, on_device(): pl.pallas_call(functools.partial(kernel, n_fs, n_tp), out_shape=(jax.Shap...  238 us
    unnamed x10, local copies, waits for them, and re-layouts  13.9 us

profile of v1, /device:TPU:0, one launch (start us, length us, event | category | flops | bytes accessed | tf_op | source)
XLA Modules:
  0.0 253.8 jit_solution(14322542519374964896)
XLA Ops:
  0.6 1.5 copy.9.gain
  2.1 237.8 %shard_map.84 = (bf16[2048,1408]{1,0:T(8,128)(2,1)}, bf16[2048,1408]{1,0:T(8,128)(2,1)}, bf16[1408,2048]{1,0:T(8,128)(2,1)}, bf16[768,512]{1,0:T(8,128)(2,1)}) custom-call(bf16[768,2048]{1,0:T(8,128)(2,1)} %tok.1, f32[256,1]{1,0:T(8,128)} %copy.9.gain, f32[256,1408]{1,0:T(8,128)} %gw.1, f32[256,1408]{1,0:T(8,128)} %uw.1, f32[704,512]{1,0:T(8,128)} %dw.1), custom_call_target="tpu_custom_call" | custom-call | tf_op jit(solution)/shard_map/pallas_call | solution.py:317
  240.0 0.0 copy-start.1
  240.0 5.7 %copy.14 = bf16[2048,1408]{1,0:T(8,128)(2,1)} copy(bf16[2048,1408]{1,0:T(8,128)(2,1)} %get-tuple-element.8) | data formatting | bytes 11534336
  245.7 0.0 copy-done.1
  245.7 0.0 copy-start
  245.7 2.9 %copy.15 = bf16[2048,1408]{1,0:T(8,128)(2,1)} copy(bf16[2048,1408]{1,0:T(8,128)(2,1)S(1)} %copy-done.1) | data formatting | bytes 11534336
  248.6 1.8 copy-done
  250.4 0.0 copy-start.2
  250.4 2.5 copy.16
  253.0 0.0 copy-done.2
  253.0 0.9 copy.17
Async XLA Ops:
  240.0 5.8 %copy-start.1 = (bf16[2048,1408]{1,0:T(8,128)(2,1)S(1)}, bf16[2048,1408]{1,0:T(8,128)(2,1)}, u32[]{:S(2)}) copy-start(bf16[2048,1408]{1,0:T(8,128)(2,1)} %get-tuple-element.9) | copy-start | bytes 17301508
  245.7 4.7 %copy-start = (bf16[1408,2048]{1,0:T(8,128)(2,1)S(1)}, bf16[1408,2048]{1,0:T(8,128)(2,1)}, u32[]{:S(2)}) copy-start(bf16[1408,2048]{1,0:T(8,128)(2,1)} %get-tuple-element.10) | copy-start | bytes 17301508
  250.4 2.5 copy-start.2

commit v2 on v1

v2 whole, which is shorter than its diff:
```python
import functools

import jax
import jax.numpy as jnp
from jax import lax
from jax.experimental import pallas as pl
from jax.experimental.pallas import tpu as pltpu
from jax.sharding import PartitionSpec as P

eps_norm = 1e-06
MESH = pl.DeviceIdType.MESH

PIECES = (
    ("gate", 0, 1, "a"),
    ("gate", 1, 1, "a"),
    ("down", 2, 2, "b"),
    ("up", 0, 1, "a"),
    ("up", 1, 1, "a"),
    ("down", 0, 1, "a"),
    ("down", 1, 1, "a"),
)
PHASES = ((0, 1, 6), (2,), (3, 4), (5,))
GROUPS = ((1, 3, (2, 6)), (0, 1, (5,)))


def cost(p):
    return 0.5 if PIECES[p][0] == "down" and kind(p) == 1 else 1.0


def kind(p):
    return PIECES[p][3]


def plan(n_z):
    events = []
    seq = [(d, p) for phase in PHASES for d in range(1, n_z) for p in phase]
    order = sorted(range(len(PIECES)), key=lambda p: kind(p) == "a")
    own, total = {}, 0.0
    for p in order:
        total += cost(p)
        own[p] = total
    z_time, now = {}, 0.0
    for i, phase in enumerate(PHASES):
        for d in range(1, n_z):
            if d == n_z - 1 and i + 1 < len(PHASES):
                events.append((now + 0.02, 1, "launch", i + 1, 0))
            for p in phase:
                if kind(p) == "a":
                    now += cost(p)
                    z_time[d, p] = now
                    events.append((now, 0, "line", d, p))
                else:
                    now += 2.0 * cost(p)
                    z_time[d, p] = now
                    events.append((now - cost(p), 0, "line", d, p))
                    events.append((now, 0, "line_other", d, p))
    y_time = {}
    for z in range(n_z):
        at = total
        for d, p in seq:
            if kind(p) == "a":
                for zz in (z - d, z + d):
                    if 0 <= zz < n_z:
                        at = max(at, z_time[d, p]) + cost(p)
                        y_time[d, p] = max(y_time.get((d, p), 0.0), at)
    for p, at in own.items():
        events.append((at, 1, "pair", 0, p))
    for (d, p), at in y_time.items():
        events.append((at, 1, "pair", d, p))
    here = dict(y_time)
    here.update({(0, p): at for p, at in own.items()})
    last = 0.0
    for name in ("gate", "up"):
        mine = [p for p in range(len(PIECES)) if PIECES[p][0] == name]
        for d in range(n_z):
            at = max(here[d, p] for p in mine) + 0.01
            events.append((at, 2, "mul_" + name, d, 0))
            last = max(last, at)
    events.append((last + 0.01, 3, "act", 0, 0))
    end = max(e[0] for e in events) + 0.1
    for step in range(4):
        events.append((end + 0.01 + 0.01 * step, 4, "share", 0, step))
    for step in range(5):
        events.append((end + 0.1 + 0.1 * step, 4, "share", 1, step))
    events.append((end + 0.35, 4, "share", 0, 4))
    return sorted(events)


def kernel(
    n_fs, n_tp, tok_hbm, gain, gw, uw, dw, gate_o, up_o, down_o, mix_o,
    tok, dcol, normed, acc_g, acc_u, hidden, share0, share1, pair0, pair1, send0, send1, in0, in1,
    tok_sem, ag_send, ag_recv, aa_send, aa_recv, rs_send, rs_recv,
):
    tok_copy = pltpu.make_async_copy(tok_hbm, tok, tok_sem)
    tok_copy.start()
    shares, pairs, sends, ins = (share0, share1), (pair0, pair1), (send0, send1), (in0, in1)
    f, t = lax.axis_index("fs"), lax.axis_index("tp")
    n_z = n_fs // 2
    z, y = f // 2, f % 2
    per = n_fs // n_tp
    rows = gw.shape[0]
    d_rows, d_cols = dw.shape
    part = d_cols // 4
    n_tok = tok.shape[0]
    k_z = normed.shape[2]
    m_tile = min(256, n_tok)
    width = gw.shape[1]
    col_tiles = [(c, min(512, width - c)) for c in range(0, width, 512)]

    def flip(bit):
        return t + bit - 2 * bit * ((t // bit) % 2)

    near, far = flip(1), flip(2)
    far_near = far + 1 - 2 * (far % 2)

    def view(o, p):
        name, h, n, _ = PIECES[p]
        if name == "down":
            return dcol.at[o, :, pl.ds(h * part, n * part)]
        ref = gate_o if name == "gate" else up_o
        return ref.at[pl.ds(pl.multiple_of(o * rows + h * (rows // 2), rows // 2), rows // 2), :]

    def ag(o, p, way, dest):
        v = view(o, p)
        return pltpu.make_async_remote_copy(
            v, v, ag_send.at[o, p, way], ag_recv.at[o, p],
            device_id=(dest, t), device_id_type=MESH,
        )

    started = []

    def start(cond, make):
        if cond is None:
            make().start()
        else:
            pl.when(cond)(lambda: make().start())
        started.append((cond, make))

    def land(o, p):
        ag(o, p, 0, f).wait_recv()

    def exchange(cond, o, p):
        name, h, n, _ = PIECES[p]
        if name != "down":
            return
        owner = o // per
        k = o % per
        row = pl.multiple_of(k * d_rows, d_rows)
        col = pl.multiple_of(t * d_cols + h * part, part)

        def make():
            return pltpu.make_async_remote_copy(
                view(o, p), down_o.at[pl.ds(row, d_rows), pl.ds(col, n * part)],
                aa_send.at[o, p], aa_recv.at[t, k, p],
                device_id=(f, owner), device_id_type=MESH,
            )

        away = owner != t
        start(away if cond is None else jnp.logical_and(cond, away), make)
        mine = owner == t

        @pl.when(mine if cond is None else jnp.logical_and(cond, mine))
        def _():
            down_o[pl.ds(row, d_rows), pl.ds(col, n * part)] = dcol[o, :, h * part : (h + n) * part]

    barrier = pltpu.get_barrier_semaphore()
    other_y = f + 1 - 2 * y
    peers = [
        (z > 0, (f - 2, t)), (z < n_z - 1, (f + 2, t)), (None, (other_y, t)),
        (None, (f, near)), (None, (f, far)), (None, (f, far_near)),
    ]
    for cond, dev in peers:
        def hello(dev=dev):
            pl.semaphore_signal(barrier, inc=1, device_id=dev, device_id_type=MESH)
        hello() if cond is None else pl.when(cond)(hello)

    g = jnp.broadcast_to(gain[...], (8, rows)).T[:, :1]
    base = pl.multiple_of(f * rows, rows)
    gate_o[pl.ds(base, rows), :] = (gw[...] * g).astype(jnp.bfloat16)
    dcol[f] = dw[...].astype(jnp.bfloat16)
    up_o[pl.ds(base, rows), :] = (uw[...] * g).astype(jnp.bfloat16)
    inner = jnp.logical_and(z > 0, z < n_z - 1)
    pl.when(inner)(lambda: pl.semaphore_wait(barrier, len(peers)))
    pl.when(jnp.logical_not(inner))(lambda: pl.semaphore_wait(barrier, len(peers) - 1))

    def launch(phase):
        for p in PHASES[phase]:
            start(z > 0, functools.partial(ag, f, p, 0, f - 2))
            start(z < n_z - 1, functools.partial(ag, f, p, 1, f + 2))
            if kind(p) == "b":
                other_b(p)

    def other_b(p):
        start(z > 0, functools.partial(ag, other_y, p, 0, f - 2))
        start(z < n_z - 1, functools.partial(ag, other_y, p, 1, f + 2))

    for p in sorted(range(len(PIECES)), key=lambda p: kind(p) == "a"):
        start(None, functools.partial(ag, f, p, 2, other_y))
    for p in PHASES[0]:
        start(z > 0, functools.partial(ag, f, p, 0, f - 2))
        start(z < n_z - 1, functools.partial(ag, f, p, 1, f + 2))
    for p in range(len(PIECES)):
        exchange(None, f, p)

    n_norm = n_tok // 64
    tok_copy.wait()

    @pl.loop(0, n_norm)
    def _(i):
        r = pl.multiple_of(i * 64, 64)
        x = tok[pl.ds(r, 64), :].astype(jnp.float32)
        x = x * lax.rsqrt(jnp.mean(x * x, axis=-1, keepdims=True) + eps_norm)
        x = x.astype(jnp.bfloat16)
        for j in range(n_z):
            normed[j, pl.ds(r, 64), :] = x[:, j * k_z : (j + 1) * k_z]

    def multiply(w, acc, zz, first):
        k0 = pl.multiple_of(zz * k_z, k_z)

        @pl.loop(0, n_tok // m_tile)
        def _(i):
            r = pl.multiple_of(i * m_tile, m_tile)
            a = normed[zz, pl.ds(r, m_tile), :]
            for c, n in col_tiles:
                v = jnp.dot(a, w[pl.ds(k0, k_z), c : c + n], preferred_element_type=jnp.float32)
                if first:
                    acc[pl.ds(r, m_tile), c : c + n] = v
                else:
                    acc[pl.ds(r, m_tile), c : c + n] += v

    def sides(d):
        return [(z >= d, z - d, -1), (z + d < n_z, z + d, 1)]

    def forward(cond, zz, sign, o, p):
        if sign < 0:
            start(jnp.logical_and(cond, z < n_z - 1), functools.partial(ag, o, p, 1, f + 2))
        else:
            start(jnp.logical_and(cond, z > 0), functools.partial(ag, o, p, 0, f - 2))

    def share_step(group, step):
        q, n, parts = GROUPS[group]
        share, half_in, out_send, out_in = shares[group], pairs[group], sends[group], ins[group]
        wide = n * part

        def aa_wait(c):
            for k in range(per):
                for p in parts:
                    _, h, m, _ = PIECES[p]
                    ref = down_o.at[
                        pl.ds(k * d_rows, d_rows), pl.ds(pl.multiple_of(c * d_cols + h * part, part), m * part)
                    ]
                    pltpu.make_async_remote_copy(
                        ref, ref, aa_send.at[0, p], aa_recv.at[c, k, p], device_id=(f, near), device_id_type=MESH,
                    ).wait_recv()

        def product(c, slot):
            @pl.loop(0, n_tok // m_tile)
            def _(i):
                r = pl.multiple_of(i * m_tile, m_tile)
                col = pl.multiple_of(c * d_cols + q * part, part)
                v = jnp.dot(hidden[pl.ds(r, m_tile), :], down_o[:, pl.ds(col, wide)], preferred_element_type=jnp.float32)
                share[slot, pl.ds(r, m_tile), :] = v.astype(jnp.bfloat16)

        def pair(slot):
            return pltpu.make_async_remote_copy(
                share.at[slot], half_in.at[slot], rs_send.at[group, slot], rs_recv.at[group, slot],
                device_id=(f, near), device_id_type=MESH,
            )

        def across():
            return pltpu.make_async_remote_copy(
                out_send, out_in, rs_send.at[group, 2], rs_recv.at[group, 2],
                device_id=(f, far), device_id_type=MESH,
            )

        if step == 0:
            aa_wait(far_near)
            product(far_near, 0)
            start(None, functools.partial(pair, 0))
        elif step == 1:
            aa_wait(far)
            product(far, 2)
            pair(0).wait_recv()
            out_send[...] = (share[2].astype(jnp.float32) + half_in[0].astype(jnp.float32)).astype(jnp.bfloat16)
            start(None, across)
        elif step == 2:
            aa_wait(near)
            product(near, 1)
            start(None, functools.partial(pair, 1))
        elif step == 3:
            product(t, 3)
        elif step == 4:
            pair(1).wait_recv()
            across().wait_recv()
            mix_o[:, q * part : (q + n) * part] = (
                share[3].astype(jnp.float32) + half_in[1].astype(jnp.float32) + out_in[...].astype(jnp.float32)
            ).astype(jnp.bfloat16)

    for _, _, what, d, p in plan(n_z):
        if what == "launch":
            launch(d)
        elif what == "share":
            share_step(d, p)
        elif what == "line":
            for cond, zz, sign in sides(d):
                o = zz * 2 + y
                pl.when(cond)(functools.partial(land, o, p))
                forward(cond, zz, sign, o, p)
                if kind(p) == "a":
                    start(cond, functools.partial(ag, o, p, 2, other_y))
                exchange(cond, o, p)
        elif what == "line_other":
            for cond, zz, sign in sides(d):
                o = zz * 2 + 1 - y
                pl.when(cond)(functools.partial(land, o, p))
                forward(cond, zz, sign, o, p)
                exchange(cond, o, p)
        elif what == "pair":
            if d == 0:
                land(other_y, p)
                exchange(None, other_y, p)
            else:
                for cond, zz, sign in sides(d):
                    o = zz * 2 + 1 - y
                    pl.when(cond)(functools.partial(land, o, p))
                    exchange(cond, o, p)
        elif what == "mul_gate" or what == "mul_up":
            w, acc = (gate_o, acc_g) if what == "mul_gate" else (up_o, acc_u)
            if d == 0:
                multiply(w, acc, z, True)
            else:
                for cond, zz, sign in sides(d):
                    pl.when(cond)(functools.partial(multiply, w, acc, zz, False))
        elif what == "act":
            @pl.loop(0, n_tok // 32)
            def _(i):
                r = pl.multiple_of(i * 32, 32)
                v = acc_g[pl.ds(r, 32), :]
                hidden[pl.ds(r, 32), :] = (v / (1.0 + jnp.exp(-v)) * acc_u[pl.ds(r, 32), :]).astype(jnp.bfloat16)

    for cond, make in started:
        if cond is None:
            make().wait_send()
        else:
            pl.when(cond)(lambda make=make: make().wait_send())


def on_device(n_fs, n_tp, tokens, norm_gain, gate_weight, up_weight, down_weight):
    n_tok, d_model = tokens.shape
    rows, width = gate_weight.shape
    d_rows, d_cols = down_weight.shape
    part = d_cols // 4
    n_z = n_fs // 2
    n_p = len(PIECES)
    bf = jnp.bfloat16
    vmem = pl.BlockSpec(memory_space=pltpu.VMEM)
    dma = pltpu.SemaphoreType.DMA
    return pl.pallas_call(
        functools.partial(kernel, n_fs, n_tp),
        out_shape=(
            pltpu.VMEM((d_model, width), bf),
            pltpu.VMEM((d_model, width), bf),
            pltpu.VMEM((d_rows * n_fs // n_tp, d_model), bf),
            pltpu.VMEM((n_tok, d_cols), bf),
        ),
        in_specs=[pl.BlockSpec(memory_space=pl.ANY)] + [vmem] * 4,
        out_specs=(vmem,) * 4,
        scratch_shapes=[
            pltpu.VMEM((n_tok, d_model), bf),
            pltpu.VMEM((n_fs, d_rows, d_cols), bf),
            pltpu.VMEM((n_z, n_tok, d_model // n_z), bf),
            pltpu.VMEM((n_tok, width), jnp.float32),
            pltpu.VMEM((n_tok, width), jnp.float32),
            pltpu.VMEM((n_tok, width), bf),
            *[pltpu.VMEM((4, n_tok, g[1] * part), bf) for g in GROUPS],
            *[pltpu.VMEM((2, n_tok, g[1] * part), bf) for g in GROUPS],
            *[pltpu.VMEM((n_tok, g[1] * part), bf) for g in GROUPS],
            *[pltpu.VMEM((n_tok, g[1] * part), bf) for g in GROUPS],
            dma,
            dma((n_fs, n_p, 3)),
            dma((n_fs, n_p)),
            dma((n_fs, n_p)),
            dma((n_tp, n_fs // n_tp, n_p)),
            dma((2, 3)),
            dma((2, 3)),
        ],
        compiler_params=pltpu.CompilerParams(
            collective_id=0, has_side_effects=True, vmem_limit_bytes=46 * 2**20
        ),
    )(tokens, norm_gain[None, :], gate_weight, up_weight, down_weight)


def solution(mesh):
    n_fs, n_tp = mesh.shape["fs"], mesh.shape["tp"]
    in_specs = (P("fs", None), P("fs"), P("fs", "tp"), P("fs", "tp"), P("fs", "tp"))
    out_specs = (P(None, "tp"), P(None, "tp"), P("tp", None), P("fs", "tp"))
    return jax.shard_map(
        functools.partial(on_device, n_fs, n_tp), mesh=mesh, in_specs=in_specs, out_specs=out_specs, check_vma=False
    )
```

time: 254 us -> 216 us (0.85)
  Pallas kernels: 238 us -> 207 us
  local copies, waits for them, and re-layouts: 15.4 us -> 8.47 us
    pallas_call x1, Pallas kernels: 238 us -> 207 us  [on_device(): pl.pallas_call(functools.partial(kernel, n_fs, n_tp), out_shape=(pltpu.VM...]
    unnamed x10 -> x4, local copies, waits for them, and re-layouts: 13.9 us -> 8.47 us
where the time goes in v2:
time: 216 us
  Pallas kernels  207 us (96%)
  local copies, waits for them, and re-layouts  8.47 us (4%)
    pallas_call x1, Pallas kernels, on_device(): pl.pallas_call(functools.partial(kernel, n_fs, n_tp), out_shape=(pltpu.VM...  207 us
    unnamed x4, local copies, waits for them, and re-layouts  8.47 us

profile of v2, /device:TPU:0, one launch (start us, length us, event | category | flops | bytes accessed | tf_op | source)
XLA Modules:
  0.0 216.1 jit_solution(1866270889515319469)
XLA Ops:
  0.6 207.0 %shard_map.84 = (bf16[2048,1408]{1,0:T(8,128)(2,1)S(1)}, bf16[2048,1408]{1,0:T(8,128)(2,1)S(1)}, bf16[1408,2048]{1,0:T(8,128)(2,1)S(1)}, bf16[768,512]{1,0:T(8,128)(2,1)S(1)}) custom-call(bf16[768,2048]{1,0:T(8,128)(2,1)} %tok_hbm.1, f32[1,256]{1,0:T(1,128)} %bitcast.1, f32[256,1408]{1,0:T(8,128)} %gw.1, f32[256,1408]{1,0:T(8,128)} %uw.1, f32[704,512]{1,0:T(8,128)} %dw.1), custom_call_target="tpu_custom_call" | custom-call | tf_op jit(solution)/shard_map/pallas_call | solution.py:358
  207.6 2.5 %copy.13 = bf16[2048,1408]{1,0:T(8,128)(2,1)} copy(bf16[2048,1408]{1,0:T(8,128)(2,1)S(1)} %get-tuple-element.4) | data formatting | bytes 11534336
  210.2 0.9 copy.16
  211.1 2.5 %copy.14 = bf16[2048,1408]{1,0:T(8,128)(2,1)} copy(bf16[2048,1408]{1,0:T(8,128)(2,1)S(1)} %get-tuple-element.5) | data formatting | bytes 11534336
  213.6 2.5 %copy.15 = bf16[1408,2048]{1,0:T(8,128)(2,1)} copy(bf16[1408,2048]{1,0:T(8,128)(2,1)S(1)} %get-tuple-element.6) | data formatting | bytes 11534336
